TPU v7x, 32 devices: a whole 2x2x4 slice. The times are simulated.
32 devices in a mesh: kv: 8 (over y, x, core), tp: 4 (over z).
Axes of the slice: x: 2, y: 2, z: 4, core: 2. Of those that a mesh axis runs over, the one named last changes fastest.
Arguments:
- tokens: bfloat16 [320, 4096], P('tp', 'kv'), may hold values from -8 to 8
- state: float32 [320, 32, 128, 128], P('kv', 'tp'), may hold values from -4 to 4
- mix_gain: float32 [4096], P('kv'), may hold values from 0.1 to 1.9
- q_weight: bfloat16 [4096, 4096], P('kv', 'tp'), may hold values from -0.09375 to 0.09375
- forget_weight: bfloat16 [4096, 4096], P('kv', 'tp'), may hold values from -0.09375 to 0.09375
- input_weight: bfloat16 [4096, 4096], P('kv', 'tp'), may hold values from -0.09375 to 0.09375
- gate_weight: bfloat16 [4096, 4096], P('kv', 'tp'), may hold values from -0.09375 to 0.09375
- lower_bound: float32 [4096], P('tp'), may hold values from 0 to 0.9
- head_gain: float32 [128], replicated, may hold values from 0.1 to 1.9
- out_weight: bfloat16 [4096, 4096], P('tp', 'kv'), may hold values from -0.09375 to 0.09375
- ffn_gain: float32 [4096], P('kv'), may hold values from 0.1 to 1.9
- ffn_gate: bfloat16 [4096, 10240], P('kv', 'tp'), may hold values from -0.09375 to 0.09375
- ffn_up: bfloat16 [4096, 10240], P('kv', 'tp'), may hold values from -0.09375 to 0.09375
- ffn_down: bfloat16 [10240, 4096], P('tp', 'kv'), may hold values from -0.0625 to 0.0625
Outputs:
- layer_out: bfloat16 [320, 4096], P('tp', 'kv')
- new_state: float32 [320, 32, 128, 128], P('kv', 'tp')
All inputs are finite; a program needn't handle non-finite values.
Results may differ from a plain program's by a relative error of at most 0.007.
Values may be sent and summed in bfloat16 or wider, within the bound.
A program may use at most 128 MiB of HBM per device.

v0:
```python
import functools

import jax
import jax.numpy as jnp
from jax import lax
from jax.experimental import pallas as pl
from jax.experimental.pallas import tpu as pltpu
from jax.sharding import PartitionSpec as P

EPS = 1e-05
F32 = jnp.float32
BF16 = jnp.bfloat16
LANES = 128
MESH = pl.DeviceIdType.MESH
ANY = pl.BlockSpec(memory_space=pl.ANY)
VMEM = pl.BlockSpec(memory_space=pltpu.VMEM)


def remote(src, dst, send, recv, axis, peer):
    return pltpu.make_async_remote_copy(
        src_ref=src,
        dst_ref=dst,
        send_sem=send,
        recv_sem=recv,
        device_id={axis: peer},
        device_id_type=MESH,
    )


def greet(n_kv, n_tp):
    kv, tp = lax.axis_index("kv"), lax.axis_index("tp")
    barrier = pltpu.get_barrier_semaphore()
    for axis, me, n in (("kv", kv, n_kv), ("tp", tp, n_tp)):
        for off in range(1, n):
            pl.semaphore_signal(
                barrier,
                inc=1,
                device_id={axis: lax.rem(me + off, n)},
                device_id_type=MESH,
            )
    pl.semaphore_wait(barrier, n_kv + n_tp - 2)


def partner_of(me):
    return me + 1 - 2 * lax.rem(me, 2)


def exchange_start(src_at, dst, send, recv, axis, n):
    me = lax.axis_index(axis)
    copies = []
    for off in range(1, n):
        peer = lax.rem(me + off, n)
        copy = remote(src_at(peer), dst.at[me], send.at[off], recv.at[off], axis, peer)
        copy.start()
        copies.append(copy)
    return copies


def gather_start(own, gathered, send, recv, fsend, frecv, n):
    me = lax.axis_index("kv")
    half = n // 2
    mine = me // 2
    parity = lax.rem(me, 2)
    partner = partner_of(me)
    first = []
    for off in range(1, half):
        peer = lax.rem(mine + off, half) * 2 + parity
        copy = remote(own, gathered.at[me], send.at[off], recv.at[off], "kv", peer)
        copy.start()
        first.append(copy)
    pair = remote(own, gathered.at[me], fsend.at[0], frecv.at[0], "kv", partner)
    pair.start()
    gathered[me] = own[...]
    return first, pair


def gather_finish(started, gathered, fsend, frecv, n):
    first, pair = started
    me = lax.axis_index("kv")
    half = n // 2
    mine = me // 2
    parity = lax.rem(me, 2)
    partner = partner_of(me)
    second = [pair]
    for off in range(1, half):
        first[off - 1].wait_recv()
        source = lax.rem(mine + half - off, half) * 2 + parity
        copy = remote(
            gathered.at[source], gathered.at[source], fsend.at[off], frecv.at[off], "kv", partner
        )
        copy.start()
        second.append(copy)
    for copy in second:
        copy.wait_recv()
    return first + second


class Scatter:
    def __init__(self, refs, n):
        (self.out, self.pair_in, self.mid, self.rest_in, self.ps, self.pr, self.rs, self.rr) = refs
        self.n = n
        self.half = n // 2
        self.me = lax.axis_index("kv")
        self.mine = self.me // 2
        self.parity = lax.rem(self.me, 2)
        self.pairs = []
        self.rests = []

    def put(self, c, cols, block):
        rows = block.shape[0] // self.n
        for j in range(self.n):
            self.out[c, j % 2, j // 2, :, cols] = block[j * rows : (j + 1) * rows].astype(BF16)

    def send_pair(self, c):
        copy = remote(
            self.out.at[c, 1 - self.parity],
            self.pair_in.at[c],
            self.ps.at[c],
            self.pr.at[c],
            "kv",
            partner_of(self.me),
        )
        copy.start()
        self.pairs.append(copy)

    def pair_sum(self, c, j):
        return self.out[c, self.parity, j].astype(F32) + self.pair_in[c, j].astype(F32)

    def send_rest(self, c):
        self.pairs[c].wait_recv()
        copies = []
        for off in range(1, self.half):
            j = lax.rem(self.mine + off, self.half)
            self.mid[c, off] = self.pair_sum(c, j).astype(BF16)
            copy = remote(
                self.mid.at[c, off],
                self.rest_in.at[c, off],
                self.rs.at[c, off],
                self.rr.at[c, off],
                "kv",
                j * 2 + self.parity,
            )
            copy.start()
            copies.append(copy)
        self.rests.append(copies)

    def total(self, c):
        for copy in self.rests[c]:
            copy.wait_recv()
        total = self.pair_sum(c, self.mine)
        for off in range(1, self.half):
            total = total + self.rest_in[c, off].astype(F32)
        return total

    def close(self):
        for copy in self.pairs:
            copy.wait_send()
        for copies in self.rests:
            for copy in copies:
                copy.wait_send()


def scatter_scratch(chunks, n, rows, cols):
    half = n // 2
    return [
        pltpu.VMEM((chunks, 2, half, rows, cols), BF16),
        pltpu.VMEM((chunks, half, rows, cols), BF16),
        pltpu.VMEM((chunks, half, rows, cols), BF16),
        pltpu.VMEM((chunks, half, rows, cols), BF16),
        pltpu.SemaphoreType.DMA((chunks,)),
        pltpu.SemaphoreType.DMA((chunks,)),
        pltpu.SemaphoreType.DMA((chunks, half)),
        pltpu.SemaphoreType.DMA((chunks, half)),
    ]


def squares_scratch(n, rows):
    return [
        pltpu.VMEM((n, rows, LANES), F32),
        pltpu.VMEM((n, rows, LANES), F32),
        pltpu.SemaphoreType.DMA((n,)),
        pltpu.SemaphoreType.DMA((n,)),
    ]


def squares_start(values, refs, n):
    out, into, send, recv = refs
    totals = jnp.sum(values * values, axis=1, keepdims=True)
    totals = jnp.broadcast_to(totals, (values.shape[0], LANES))
    out[...] = totals.reshape(out.shape)
    return exchange_start(lambda peer: out.at[peer], into, send, recv, "kv", n)


def squares_factor(copies, refs, n, width):
    out, into, _, _ = refs
    me = lax.axis_index("kv")
    for copy in copies:
        copy.wait_recv()
    total = out[me]
    for off in range(1, n):
        total = total + into[lax.rem(me + off, n)]
    return lax.rsqrt(total[:, :1] / width + EPS)


def tile_of(cols):
    return 512 if cols % 512 == 0 else cols


def mixer_in(n_kv, n_tp, width, tokens, gain, wq, wf, wv, wg, sums, rows_all, weights, *rest):
    scatter_refs, square_refs = rest[:8], rest[8:12]
    load_sem, t_send, t_recv = rest[12:]
    tp = lax.axis_index("tp")
    loads = [
        pltpu.make_async_copy(w, weights.at[i], load_sem.at[i])
        for i, w in enumerate((wq, wf, wv, wg))
    ]
    for load in loads:
        load.start()
    greet(n_kv, n_tp)
    copies = exchange_start(lambda peer: tokens, rows_all, t_send, t_recv, "tp", n_tp)
    rows_all[tp] = tokens[...]
    for copy in copies:
        copy.wait_recv()
    batch = n_tp * tokens.shape[0]
    values = rows_all[...].astype(F32).reshape(batch, tokens.shape[1])
    normed = (values * gain[...]).astype(BF16)
    scatter = Scatter(scatter_refs, n_kv)
    cols = weights.shape[2]
    tile = tile_of(cols)
    squares = None
    for c in range(4):
        loads[c].wait()
        for at in range(0, cols, tile):
            part = pl.ds(at, tile)
            scatter.put(
                c, part, jnp.dot(normed, weights[c, :, part], preferred_element_type=F32)
            )
        scatter.send_pair(c)
        if c > 0:
            scatter.send_rest(c - 1)
        if c == 0:
            squares = squares_start(values, square_refs, n_kv)
    scatter.send_rest(3)
    factor = squares_factor(squares, square_refs, n_kv, width)
    for c in range(4):
        sums[:, c * cols : (c + 1) * cols] = scatter.total(c) * factor
    for copy in copies + squares:
        copy.wait_send()
    scatter.close()


def state_step(q_pre, f_pre, v_pre, g_pre, bound, head_gain, state, new_state, gated, read):
    rows = q_pre.shape[0]
    size = state.shape[-1]
    low = bound[...]
    query = jax.nn.silu(q_pre[...]) * size ** (-0.5)
    forget = low + (1.0 - low) * jax.nn.sigmoid(f_pre[...])
    query_t = query.T
    forget_t = forget.T
    value = v_pre[...]
    for b in range(rows):
        v = value[b : b + 1, :]
        new = v + forget_t[:, b : b + 1] * (state[b, 0] - v)
        new_state[b, 0] = new
        read[b : b + 1, :] = jnp.sum(query_t[:, b : b + 1] * new, axis=0, keepdims=True)
    out = read[...]
    out = out * lax.rsqrt(jnp.mean(out * out, axis=1, keepdims=True) + EPS) * head_gain[...]
    gated[...] = (out * jax.nn.silu(g_pre[...])).astype(BF16)


def rest_of_layer(
    n_kv, n_tp, width, chunks, tokens, gated, gain, w_out, w_gate, w_up, w_down, out, *refs
):
    (v_out, v_ffn, v_down, g_all, h_own, h_all, t_acc, t_send_buf, t_recv_buf, r_own, r_all) = refs[:11]
    scatter_refs, square_refs = refs[11:19], refs[19:23]
    (load_sem, gs, gr, gfs, gfr, hs, hr, hfs, hfr, ts, tr) = refs[23:]
    tp = lax.axis_index("tp")
    loads = [
        pltpu.make_async_copy(w_out, v_out, load_sem.at[0]),
        pltpu.make_async_copy(w_gate, v_ffn.at[0], load_sem.at[1]),
        pltpu.make_async_copy(w_up, v_ffn.at[1], load_sem.at[2]),
        pltpu.make_async_copy(w_down, v_down, load_sem.at[3]),
    ]
    for load in loads:
        load.start()
    greet(n_kv, n_tp)
    done = []
    rows_tp = tokens.shape[0]

    wide = tokens.shape[1] // 2
    batch = n_tp * rows_tp

    def flat(block):
        return block.astype(F32).reshape(batch, block.shape[2]).astype(BF16)

    def terms_start(k, product):
        product = product.reshape(n_tp, rows_tp, wide)
        t_acc[k] = product
        t_send_buf[k] = product.astype(BF16)
        copies = exchange_start(
            lambda peer: t_send_buf.at[k, peer], t_recv_buf.at[k], ts.at[k], tr.at[k], "tp", n_tp
        )
        done.extend(copies)
        return copies

    def terms_total(k, copies):
        total = t_acc[k, tp]
        for off in range(1, n_tp):
            copies[off - 1].wait_recv()
            total = total + t_recv_buf[k, lax.rem(tp + n_tp - off, n_tp)].astype(F32)
        return total

    started = gather_start(gated, g_all, gs, gr, gfs, gfr, n_kv)
    done.extend(gather_finish(started, g_all, gfs, gfr, n_kv))
    loads[0].wait()
    heads_in = flat(g_all[...])
    sides = [pl.ds(k * wide, wide) for k in range(2)]
    terms = [
        terms_start(k, jnp.dot(heads_in, v_out[:, sides[k]], preferred_element_type=F32))
        for k in range(2)
    ]
    gathers = []
    for k in range(2):
        attended = terms_total(k, terms[k])
        r_own[k] = (tokens[:, sides[k]].astype(F32) + attended).astype(BF16)
        gathers.append(
            exchange_start(
                lambda peer: r_own.at[k], r_all.at[k], ts.at[4 + k], tr.at[4 + k], "tp", n_tp
            )
        )
        r_all[k, tp] = r_own[k]
    for copies in gathers:
        for copy in copies:
            copy.wait_recv()
        done.extend(copies)
    values = jnp.concatenate(
        [r_all[k].astype(F32).reshape(batch, wide) for k in range(2)], axis=1
    )
    normed = (values * gain[...]).astype(BF16)
    scatter = Scatter(scatter_refs, n_kv)
    cols = v_ffn.shape[2]
    step = cols // chunks
    tile = next(t for t in (640, 512, 256, 128) if step % t == 0)
    order = [(w, h) for h in range(chunks) for w in range(2)]
    loads[1].wait()
    loads[2].wait()
    squares = None
    for c, (w, h) in enumerate(order):
        for at in range(0, step, tile):
            product = jnp.dot(
                normed, v_ffn[w, :, pl.ds(h * step + at, tile)], preferred_element_type=F32
            )
            scatter.put(c, pl.ds(at, tile), product)
        scatter.send_pair(c)
        if c > 0:
            scatter.send_rest(c - 1)
        if c == 0:
            squares = squares_start(values, square_refs, n_kv)
    scatter.send_rest(2 * chunks - 1)
    factor = squares_factor(squares, square_refs, n_kv, width)
    done.extend(squares)
    started = []
    for h in range(chunks):
        gate = scatter.total(2 * h) * factor
        up = scatter.total(2 * h + 1) * factor
        h_own[h] = (jax.nn.silu(gate) * up).astype(BF16)
        started.append(
            gather_start(
                h_own.at[h], h_all.at[h], hs.at[h], hr.at[h], hfs.at[h], hfr.at[h], n_kv
            )
        )
    loads[3].wait()
    product = None
    for h in range(chunks):
        done.extend(gather_finish(started[h], h_all.at[h], hfs.at[h], hfr.at[h], n_kv))
        piece = jnp.dot(
            flat(h_all[h]), v_down[pl.ds(h * step, step), :], preferred_element_type=F32
        )
        product = piece if product is None else product + piece
    terms = [terms_start(2 + k, product[:, k * wide : (k + 1) * wide]) for k in range(2)]
    for k in range(2):
        down = terms_total(2 + k, terms[k])
        out[:, sides[k]] = (r_own[k].astype(F32) + down).astype(BF16)
    for copy in done:
        copy.wait_send()
    scatter.close()


def body(
    n_kv,
    n_tp,
    tokens,
    state,
    mix_gain,
    q_weight,
    forget_weight,
    input_weight,
    gate_weight,
    lower_bound,
    head_gain,
    out_weight,
    ffn_gain,
    ffn_gate,
    ffn_up,
    ffn_down,
):
    rows_tp, feats = tokens.shape
    width = feats * n_kv
    rows_kv, heads, size = state.shape[:3]
    cols = q_weight.shape[1]
    ff = ffn_gate.shape[1]
    dma = pltpu.SemaphoreType.DMA
    sums = pl.pallas_call(
        functools.partial(mixer_in, n_kv, n_tp, width),
        out_shape=jax.ShapeDtypeStruct((rows_kv, 4 * cols), F32),
        in_specs=[VMEM, VMEM, ANY, ANY, ANY, ANY],
        out_specs=VMEM,
        scratch_shapes=[
            pltpu.VMEM((n_tp, rows_tp, feats), BF16),
            pltpu.VMEM((4, feats, cols), BF16),
            *scatter_scratch(4, n_kv, rows_kv, cols),
            *squares_scratch(n_kv, rows_kv),
            dma((4,)),
            dma((n_tp,)),
            dma((n_tp,)),
        ],
        compiler_params=pltpu.CompilerParams(collective_id=0, has_side_effects=True),
        name="mixer_in",
    )(tokens, mix_gain[None, :], q_weight, forget_weight, input_weight, gate_weight)

    def part(i):
        return pl.BlockSpec((rows_kv, size), lambda h: (0, i * heads + h))

    state_block = pl.BlockSpec((rows_kv, 1, size, size), lambda h: (0, h, 0, 0))
    new_state, gated = pl.pallas_call(
        state_step,
        out_shape=(
            jax.ShapeDtypeStruct(state.shape, F32),
            jax.ShapeDtypeStruct((rows_kv, cols), BF16),
        ),
        grid=(heads,),
        in_specs=[
            part(0),
            part(1),
            part(2),
            part(3),
            pl.BlockSpec((1, size), lambda h: (0, h)),
            pl.BlockSpec((1, size), lambda h: (0, 0)),
            state_block,
        ],
        out_specs=(state_block, pl.BlockSpec((rows_kv, size), lambda h: (0, h))),
        scratch_shapes=[pltpu.VMEM((rows_kv, size), F32)],
        compiler_params=pltpu.CompilerParams(dimension_semantics=("arbitrary",)),
        name="state_step",
    )(sums, sums, sums, sums, lower_bound[None, :], head_gain[None, :], state)

    half = n_kv // 2
    chunks = 2 if ff % (2 * LANES) == 0 else 1
    layer_out = pl.pallas_call(
        functools.partial(rest_of_layer, n_kv, n_tp, width, chunks),
        out_shape=jax.ShapeDtypeStruct(tokens.shape, BF16),
        in_specs=[VMEM, VMEM, VMEM, ANY, ANY, ANY, ANY],
        out_specs=VMEM,
        scratch_shapes=[
            pltpu.VMEM((cols, feats), BF16),
            pltpu.VMEM((2, feats, ff), BF16),
            pltpu.VMEM((ff, feats), BF16),
            pltpu.VMEM((n_kv, rows_kv, cols), BF16),
            pltpu.VMEM((chunks, rows_kv, ff // chunks), BF16),
            pltpu.VMEM((chunks, n_kv, rows_kv, ff // chunks), BF16),
            pltpu.VMEM((4, n_tp, rows_tp, feats // 2), F32),
            pltpu.VMEM((4, n_tp, rows_tp, feats // 2), BF16),
            pltpu.VMEM((4, n_tp, rows_tp, feats // 2), BF16),
            pltpu.VMEM((2, rows_tp, feats // 2), BF16),
            pltpu.VMEM((2, n_tp, rows_tp, feats // 2), BF16),
            *scatter_scratch(2 * chunks, n_kv, rows_kv, ff // chunks),
            *squares_scratch(n_kv, rows_kv),
            dma((4,)),
            *[dma((half,)) for _ in range(4)],
            *[dma((chunks, half)) for _ in range(4)],
            dma((6, n_tp)),
            dma((6, n_tp)),
        ],
        compiler_params=pltpu.CompilerParams(collective_id=1, has_side_effects=True),
        name="rest_of_layer",
    )(tokens, gated, ffn_gain[None, :], out_weight, ffn_gate, ffn_up, ffn_down)
    return (layer_out, new_state)


def solution(mesh):
    in_specs = (
        P("tp", "kv"),
        P("kv", "tp", None, None),
        P("kv"),
        P("kv", "tp"),
        P("kv", "tp"),
        P("kv", "tp"),
        P("kv", "tp"),
        P("tp"),
        P(),
        P("tp", "kv"),
        P("kv"),
        P("kv", "tp"),
        P("kv", "tp"),
        P("tp", "kv"),
    )
    out_specs = (P("tp", "kv"), P("kv", "tp", None, None))
    step = functools.partial(body, mesh.shape["kv"], mesh.shape["tp"])
    return jax.shard_map(step, mesh=mesh, in_specs=in_specs, out_specs=out_specs, check_vma=False)
```

profile of v0, /device:TPU:0, one launch (start us, length us, event | category | flops | bytes accessed | tf_op | source)
XLA Modules:
  0.0 128.5 jit_solution(17332949930972263247)
XLA Ops:
  0.6 33.6 %mixer_in.1.q_pre.f_pre.v_pre.g_pre = f32[40,4096]{1,0:T(8,128)} custom-call(bf16[80,512]{1,0:T(8,128)(2,1)} %tokens.3, f32[1,512]{1,0:T(1,128)} %bitcast.5, bf16[512,1024]{1,0:T(8,128)(2,1)} %wq.1, bf16[512,1024]{1,0:T(8,128)(2,1)} %wf.1, bf16[512,1024]{1,0:T(8,128)(2,1)} %wv.1, bf16[512,1024]{1,0:T(8,128)(2,1)} %wg.1), custom_call_target="tpu_custom_call" | custom-call | tf_op jit(solution)/shard_map/mixer_in/pallas_call | solution.py:413
  34.2 20.8 %state_step.1 = (f32[40,8,128,128]{3,2,1,0:T(8,128)}, bf16[40,1024]{1,0:T(8,128)(2,1)}) custom-call(f32[40,4096]{1,0:T(8,128)} %mixer_in.1.q_pre.f_pre.v_pre.g_pre, f32[40,4096]{1,0:T(8,128)} %mixer_in.1.q_pre.f_pre.v_pre.g_pre, f32[40,4096]{1,0:T(8,128)} %mixer_in.1.q_pre.f_pre.v_pre.g_pre, f32[40,4096]{1,0:T(8,128)} %mixer_in.1.q_pre.f_pre.v_pre.g_pre, ...), custom_call_target="tpu_custom_call" | custom-call | tf_op jit(solution)/shard_map/state_step/pallas_call | solution.py:435
  55.0 71.9 %rest_of_layer.1 = bf16[80,512]{1,0:T(8,128)(2,1)} custom-call(bf16[80,512]{1,0:T(8,128)(2,1)} %tokens.3, bf16[40,1024]{1,0:T(8,128)(2,1)} %get-tuple-element.4.gated, f32[1,512]{1,0:T(1,128)} %bitcast.6, bf16[1024,512]{1,0:T(8,128)(2,1)} %w_out.1, bf16[512,2560]{1,0:T(8,128)(2,1)} %w_gate.1, bf16[512,2560]{1,0:T(8,128)(2,1)} %w_up.1, bf16[2560,512]{1,0:T(8,128)(2,1)} %w_down.1), custom_call_target="tpu_custom_call" | custom-call | tf_op jit(solution)/shard_map/rest_of_layer/pallas_call | solution.py:459
  127.0 1.5 %copy.17 = bf16[80,512]{1,0:T(8,128)(2,1)} copy(bf16[80,512]{1,0:T(8,128)(2,1)} %rest_of_layer.1) | data formatting | bytes 163840
where the time goes:
time: 129 us
  Pallas kernels  126 us (98%)
  local copies, waits for them, and re-layouts  1.53 us (1%)
    pallas_call x1, Pallas kernels, body(): pl.pallas_call(functools.partial(rest_of_layer, n_kv, n_tp, width, chunks...  71.9 us
    pallas_call x1, Pallas kernels, body(): pl.pallas_call(functools.partial(mixer_in, n_kv, n_tp, width), out_shape=...  33.6 us
    pallas_call x1, Pallas kernels, body(): pl.pallas_call(state_step, out_shape=(jax.ShapeDtypeStruct(state.shape, F...  20.8 us

commit v1 on v0

v1 whole, which is shorter than its diff:
```python
import functools

import jax
import jax.numpy as jnp
from jax import lax
from jax.experimental import pallas as pl
from jax.experimental.pallas import tpu as pltpu
from jax.sharding import PartitionSpec as P

EPS = 1e-05
F32 = jnp.float32
BF16 = jnp.bfloat16
LANES = 128
SUB = 8
SLOTS = 3
MESH = pl.DeviceIdType.MESH
ANY = pl.BlockSpec(memory_space=pl.ANY)
VMEM = pl.BlockSpec(memory_space=pltpu.VMEM)


def greet(n_kv, n_tp):
    kv, tp = lax.axis_index("kv"), lax.axis_index("tp")
    barrier = pltpu.get_barrier_semaphore()
    for axis, me, n in (("kv", kv, n_kv), ("tp", tp, n_tp)):
        for off in range(1, n):
            pl.semaphore_signal(
                barrier,
                inc=1,
                device_id={axis: lax.rem(me + off, n)},
                device_id_type=MESH,
            )
    pl.semaphore_wait(barrier, n_kv + n_tp - 2)


PLANS = {
    5: (
        (1, 1, 1, 1, 1),
        (
            0, 1, 0, 2, 1, 3, 2, 4, 0, 1, 3, 0, 2, 1, 3, 0, 4, 2, 0, 1, 1, 3, 4, 2,
            0, 2, 3, 1, 0, 4, 3, 0, 2, 1, 1, 3, 4, 2, 0, 4, 2, 1, 4, 0, 2, 3, 1, 0,
            3, 4, 4, 3, 1, 2, 4, 1, 3, 0, 4, 2, 3, 2, 4, 0, 1, 3, 4, 3, 2, 4,
        ),
    ),
}


def groups_of(rows):
    if rows % SUB:
        return [(0, rows)]
    parts = PLANS[rows // SUB][0] if rows // SUB in PLANS else (rows // SUB,)
    return [(SUB * sum(parts[:i]), SUB * part) for i, part in enumerate(parts)]


def order_of(groups):
    sizes = tuple(size // SUB for _, size in groups)
    for parts, order in PLANS.values():
        if parts == sizes:
            return order
    return [i for _ in range(STEPS) for i in range(len(groups))]


STEPS = 15


def tile_of(cols):
    return next((t for t in (512, 640, 384, 256, 128) if cols % t == 0), cols)


class Layer:
    def __init__(self, dims, refs):
        self.__dict__.update(dims)
        self.__dict__.update(refs)
        self.kv = lax.axis_index("kv")
        self.tp = lax.axis_index("tp")
        self.par = lax.rem(self.kv, 2)
        self.chip = self.kv // 2
        self.partner = self.kv + 1 - 2 * self.par
        self.half = self.n_kv // 2
        self.near = (self.chip + 1 - 2 * lax.rem(self.chip, 2), lax.rem(self.chip + 2, 4))
        self.started = []
        self.sems = {}
        self.used = 0
        self.state_at = {}

    def remote(self, src, dst, axis, peer):
        i = self.used
        self.used += 1
        copy = pltpu.make_async_remote_copy(
            src_ref=src,
            dst_ref=dst,
            send_sem=self.send.at[i],
            recv_sem=self.recv.at[i],
            device_id={axis: peer},
            device_id_type=MESH,
        )
        copy.start()
        self.started.append(copy)
        return copy


    def tp_start(self, src, into, rows):
        copies = []
        for off in range(1, self.n_tp):
            peer = lax.rem(self.tp + off, self.n_tp)
            copies.append(self.remote(src, into.at[self.par, self.tp, :, rows], "tp", peer))
        pair = self.remote(src, into.at[self.par, self.tp, :, rows], "kv", self.partner)
        into[self.par, self.tp, :, rows] = src[...]
        return copies, [pair]

    def tp_relay(self, moved, into, rows):
        copies, pairs = moved
        for off in range(1, self.n_tp):
            copies[off - 1].wait_recv()
            source = lax.rem(self.tp + self.n_tp - off, self.n_tp)
            block = into.at[self.par, source, :, rows]
            pairs.append(self.remote(block, block, "kv", self.partner))


    def kv_start(self, src, into, rows):
        copies = []
        for off in range(1, self.half):
            peer = lax.rem(self.chip + off, self.half) * 2 + self.par
            copies.append(self.remote(src, into.at[self.kv, rows], "kv", peer))
        pair = self.remote(src, into.at[self.kv, rows], "kv", self.partner)
        into[self.kv, rows] = src[...]
        return copies, [pair]

    def kv_relay(self, moved, into, rows):
        copies, pairs = moved
        for off in range(1, self.half):
            copies[off - 1].wait_recv()
            source = lax.rem(self.chip + self.half - off, self.half) * 2 + self.par
            block = into.at[source, rows]
            pairs.append(self.remote(block, block, "kv", self.partner))


    def spread(self, out, into, passing, rows):
        copies = [self.remote(out.at[self.partner, rows], into.at[self.kv, rows], "kv", self.partner)]
        passed = []
        if self.square:
            ways = list(zip(self.near, self.halves(out)))
            far = pl.ds(2 * (self.half - 1 - self.chip), 2)
            for k, (chip, cols) in enumerate(ways):
                peer = 2 * chip + self.par
                passed.append(
                    self.remote(out.at[far, rows, cols], passing.at[k, :, rows], "kv", peer)
                )
            for chip, cols in ways:
                for peer in (2 * chip + self.par, 2 * chip + 1 - self.par):
                    to = into.at[self.kv, rows, cols]
                    copies.append(self.remote(out.at[peer, rows, cols], to, "kv", peer))
        else:
            for off in range(1, self.half):
                chip = lax.rem(self.chip + off, self.half) * 2
                for peer in (chip + self.par, chip + 1 - self.par):
                    copies.append(self.remote(out.at[peer, rows], into.at[self.kv, rows], "kv", peer))
        into[self.kv, rows] = out[self.kv, rows]
        return copies, passed

    def spread_on(self, sent, out, into, passing, rows):
        copies, passed = sent
        ways = list(zip(self.near[::-1], self.halves(out)))
        for k, (chip, cols) in enumerate(ways):
            passed[k].wait_recv()
            for q in range(2):
                total = out[2 * chip + q, rows, cols].astype(F32)
                out[2 * chip + q, rows, cols] = (
                    total + passing[k, q, rows].astype(F32)
                ).astype(BF16)
            for peer in (2 * chip + self.par, 2 * chip + 1 - self.par):
                to = into.at[self.kv, rows, cols]
                copies.append(self.remote(out.at[peer, rows, cols], to, "kv", peer))

    def halves(self, out):
        wide = out.shape[2] // 2
        return pl.ds(0, wide), pl.ds(wide, wide)

    def collect(self, into, rows, parity, cols):
        if self.square:
            total = into[2 * self.chip + parity, rows, cols].astype(F32)
            for chip in self.near:
                total = total + into[2 * chip + parity, rows, cols].astype(F32)
            return total
        total = into[parity, rows, cols].astype(F32)
        for i in range(1, self.half):
            total = total + into[2 * i + parity, rows, cols].astype(F32)
        return total

    def factor(self, copies, into, rows):
        for copy in copies:
            copy.wait_recv()
        total = into[0, rows]
        for i in range(1, self.half):
            total = total + into[i, rows]
        return lax.rsqrt(total[:, :1] / self.width + EPS)


    def terms_start(self, k, product, rows, size):
        product = product.reshape(self.n_tp, self.g, size, self.feats)
        self.t_acc[k, :, :, rows] = product
        self.t_out[k, :, :, rows] = product.astype(BF16)
        copies = []
        for off in range(1, self.n_tp):
            peer = lax.rem(self.tp + off, self.n_tp)
            copies.append(
                self.remote(
                    self.t_out.at[k, peer, :, rows], self.t_in.at[k, self.tp, :, rows], "tp", peer
                )
            )
        return copies

    def terms_total(self, k, copies, rows):
        total = self.t_acc[k, self.tp, :, rows]
        for off in range(1, self.n_tp):
            copies[off - 1].wait_recv()
            source = lax.rem(self.tp + self.n_tp - off, self.n_tp)
            total = total + self.t_in[k, source, :, rows].astype(F32)
        return total


    def load(self, i, src, dst):
        copy = pltpu.make_async_copy(src, dst, self.load_sem.at[i])
        copy.start()
        return copy

    def pair_load_local(self, weights, dst, at):
        mine = pl.ds(self.par * self.feats, self.feats)
        n = len(weights) // 2
        for p in range(2):

            @pl.when(self.par == p)
            def _(p=p):
                for i in range(n):
                    self.load(at + i, weights[p * n + i], dst.at[i, mine])

        return [
            pltpu.make_async_copy(weights[i], dst.at[i, mine], self.load_sem.at[at + i])
            for i in range(n)
        ]

    def pair_load_remote(self, weights, dst):
        mine = pl.ds(self.par * self.feats, self.feats)
        n = len(weights) // 2
        at = self.used
        self.used += n

        def copy(p, i):
            return pltpu.make_async_remote_copy(
                src_ref=weights[(1 - p) * n + i],
                dst_ref=dst.at[i, mine],
                send_sem=self.send.at[at + i],
                recv_sem=self.recv.at[at + i],
                device_id={"kv": self.partner},
                device_id_type=MESH,
            )

        for p in range(2):

            @pl.when(self.par == p)
            def _(p=p):
                for i in range(n):
                    copy(p, i).start()

        waits = [copy(0, i) for i in range(n)]
        self.started.extend(waits)
        return waits

    def state_load(self, c):
        slot = c % SLOTS
        rows = pl.ds(c * self.chunk, self.chunk)
        copy = pltpu.make_async_copy(
            self.state.at[rows], self.s_buf.at[slot], self.state_sem.at[slot]
        )
        copy.start()
        self.state_at[c] = copy


    def normed(self, into, rows, size):
        total = self.n_kv * size
        squares = None
        for p in range(2):
            values = into[p, :, :, rows].astype(F32).reshape(total, self.feats)
            cols = pl.ds(p * self.feats, self.feats)
            self.lhs[:total, cols] = (values * self.gains[self.which, p]).astype(BF16)
            part = jnp.sum(values * values, axis=1, keepdims=True)
            squares = part if squares is None else squares + part
        return squares

    def project(self, weights, cols, out, rows, size):
        total = self.n_kv * size
        tile = tile_of(cols)
        per = cols // tile
        n = weights.shape[0]

        def step(t, carry):
            i, at = t // per, pl.multiple_of(lax.rem(t, per) * tile, LANES)
            product = jnp.dot(
                self.lhs[:total, :], weights[i, :, pl.ds(at, tile)], preferred_element_type=F32
            )
            to = pl.multiple_of(t * tile, LANES)
            out[:, rows, pl.ds(to, tile)] = product.reshape(self.n_kv, size, tile).astype(BF16)
            return carry

        [step(t, 0) for t in range(n * per)]

    def flat(self, block, size):
        return block.astype(F32).reshape(self.n_kv * size, block.shape[2]).astype(BF16)

    def read_state(self, rows, size):
        n = self.head_size
        shape = (self.heads, self.heads * n)
        own = lax.broadcasted_iota(jnp.int32, shape, 0) == (
            lax.broadcasted_iota(jnp.int32, shape, 1) // n
        )
        for c in range(rows.start // self.chunk, (rows.start + size) // self.chunk):
            self.state_at[c].wait()
            slot = c % SLOTS
            here = pl.ds(c * self.chunk, self.chunk)

            for b in range(self.chunk):
                at = pl.ds(c * self.chunk + b, 1)
                qf = self.qf[at]
                high = qf.astype(BF16).astype(F32)
                parts = jnp.concatenate(
                    [jnp.where(own, high, 0.0), jnp.where(own, qf - high, 0.0)], axis=0
                )
                kept = self.s_buf[slot, b].reshape(self.heads * n, n).astype(BF16)
                seen = jnp.dot(parts.astype(BF16), kept, preferred_element_type=F32)
                self.seen[at] = (seen[: self.heads] + seen[self.heads :])[None]
            if c + SLOTS < self.chunks:
                self.state_load(c + SLOTS)
        for h in range(self.heads):
            cols = pl.ds(h * n, n)
            rest = jnp.sum(self.qv[rows, cols], axis=1, keepdims=True)
            seen = self.seen[rows, h] + rest * self.fv[1, rows, cols]
            seen = seen * lax.rsqrt(jnp.mean(seen * seen, axis=1, keepdims=True) + EPS)
            seen = seen * self.head_gain[...]
            self.gated[rows, cols] = (seen * self.opened[rows, cols]).astype(BF16)


    def stages(self, rows, size):
        cols = self.cols
        tokens_at = self.tokens.at[:, rows]

        moved = self.tp_start(tokens_at, self.x_all, rows)
        yield
        self.tp_relay(moved, self.x_all, rows)
        yield
        for copy in moved[1]:
            copy.wait_recv()
        self.ready("mixer")
        self.which = 0
        squares = self.normed(self.x_all, rows, size)
        self.project(self.w_mix, cols, self.m_out, rows, size)
        sent = self.spread(self.m_out, self.m_in, self.m_pass, rows)
        summed = self.squares_send(squares, 0, rows, size)
        yield
        self.then("mixer")
        if self.square:
            self.spread_on(sent, self.m_out, self.m_in, self.m_pass, rows)
            yield
        for copy in sent[0]:
            copy.wait_recv()
        factor = self.factor(summed, self.q_in.at[0], rows)
        low = self.low[...]
        size_k = self.head_size
        first, second = pl.ds(0, cols), pl.ds(cols, cols)
        query = jax.nn.silu(self.collect(self.m_in, rows, 0, first) * factor) * size_k ** (-0.5)
        forget = low + (1.0 - low) * jax.nn.sigmoid(
            self.collect(self.m_in, rows, 0, second) * factor
        )
        self.fv[0, rows] = forget
        self.qf[rows] = query * forget
        self.qv[rows] = query * (1.0 - forget)
        self.fv[1, rows] = self.collect(self.m_in, rows, 1, first) * factor
        self.opened[rows] = jax.nn.silu(self.collect(self.m_in, rows, 1, second) * factor)
        self.read_state(rows, size)
        moved = self.kv_start(self.gated.at[rows], self.g_all, rows)
        yield
        self.kv_relay(moved, self.g_all, rows)
        yield
        for copy in moved[1]:
            copy.wait_recv()
        self.ready("out")
        product = jnp.dot(
            self.flat(self.g_all[:, rows], size), self.w_out_v[...], preferred_element_type=F32
        )
        terms = self.terms_start(0, product, rows, size)
        yield
        attended = self.terms_total(0, terms, rows)
        self.res[:, rows] = (self.tokens[:, rows].astype(F32) + attended).astype(BF16)
        moved = self.tp_start(self.res.at[:, rows], self.r_all, rows)
        yield
        self.tp_relay(moved, self.r_all, rows)
        yield
        for copy in moved[1]:
            copy.wait_recv()
        self.ready("ffn")
        self.which = 1
        squares = self.normed(self.r_all, rows, size)
        self.project(self.w_ffn, self.ff, self.f_out, rows, size)
        sent = self.spread(self.f_out, self.f_in, self.f_pass, rows)
        summed = self.squares_send(squares, 1, rows, size)
        yield
        if self.square:
            self.spread_on(sent, self.f_out, self.f_in, self.f_pass, rows)
            yield
        for copy in sent[0]:
            copy.wait_recv()
        factor = self.factor(summed, self.q_in.at[1], rows)
        every = pl.ds(0, self.ff)
        gate = self.collect(self.f_in, rows, 0, every) * factor
        up = self.collect(self.f_in, rows, 1, every) * factor
        self.hid[rows] = (jax.nn.silu(gate) * up).astype(BF16)
        moved = self.kv_start(self.hid.at[rows], self.h_all, rows)
        yield
        self.kv_relay(moved, self.h_all, rows)
        yield
        for copy in moved[1]:
            copy.wait_recv()
        self.ready("down")
        product = jnp.dot(
            self.flat(self.h_all[:, rows], size), self.w_down_v[...], preferred_element_type=F32
        )
        terms = self.terms_start(1, product, rows, size)
        yield
        down = self.terms_total(1, terms, rows)
        self.out[:, rows] = (self.res[:, rows].astype(F32) + down).astype(BF16)

    def squares_send(self, totals, k, rows, size):
        out, into = self.q_out.at[k], self.q_in.at[k]
        totals = jnp.broadcast_to(totals, (self.n_kv * size, LANES))
        out[:, rows] = totals.reshape(self.n_kv, size, LANES)
        copies = []
        for off in range(1, self.half):
            peer = lax.rem(self.chip + off, self.half) * 2 + self.par
            copies.append(self.remote(out.at[peer, rows], into.at[self.chip, rows], "kv", peer))
        into[self.chip, rows] = out[self.kv, rows]
        return copies

    def ready(self, name):
        for copy in self.pending.pop(name, ()):
            if isinstance(copy, tuple):
                copy[0].wait_recv()
            else:
                copy.wait()

    def then(self, name):
        for start in self.later.pop(name, ()):
            start()


NAMES = (
    "tokens", "mix_gain", "ffn_gain", "low", "head_gain", "state", "wq", "wf", "wv", "wg",
    "w_out", "w_gate", "w_up", "w_down", "out", "fv", "w_mix", "w_ffn", "w_out_v", "w_down_v",
    "x_all", "r_all", "lhs", "gains", "m_out", "m_in", "f_out", "f_in", "m_pass", "f_pass", "q_out", "q_in", "qf",
    "qv", "seen", "opened", "gated", "g_all", "hid", "h_all", "t_acc", "t_out", "t_in", "res",
    "s_buf", "send", "recv", "load_sem", "state_sem",
)


def layer(dims, *refs):
    run = Layer(dims, dict(zip(NAMES, refs)))
    mix = (run.wq, run.wf, run.wv, run.wg)
    ffn = (run.w_gate, run.w_up)
    local_mix = run.pair_load_local(mix, run.w_mix, 0)
    for c in range(min(SLOTS, run.chunks)):
        run.state_load(c)
    local_out = run.load(2, run.w_out, run.w_out_v)
    local_ffn = run.pair_load_local(ffn, run.w_ffn, 3)
    local_down = run.load(4, run.w_down, run.w_down_v)
    greet(run.n_kv, run.n_tp)
    run.pending = {
        "out": [local_out],
        "down": [local_down],
        "mixer": list(local_mix),
        "ffn": list(local_ffn),
    }

    def share_gain(k, gain):
        run.gains[k, run.par] = gain[...]
        copy = run.remote(gain, run.gains.at[k, run.par], "kv", run.partner)
        run.pending[("mixer", "ffn")[k]].append((copy,))

    def share_ffn():
        for copy in run.pair_load_remote(ffn, run.w_ffn):
            run.pending["ffn"].append((copy,))

    run.later = {"mixer": [share_ffn]}
    flows = [run.stages(pl.ds(at, size), size) for at, size in dims["groups"]]
    live = {i: 0 for i in range(len(flows))}
    for flow in flows:
        next(flow)
    share_gain(0, run.mix_gain)
    share_gain(1, run.ffn_gain)
    for copy in run.pair_load_remote(mix, run.w_mix):
        run.pending["mixer"].append((copy,))
    for i in dims["order"]:
        next(flows[i], None)
    for copy in run.started:
        copy.wait_send()


def state_step(fv, layer_in, state, new_state, layer_out):
    n, heads, size = state.shape[:3]
    shape = (3 * n, n * size)
    own = lax.rem(lax.broadcasted_iota(jnp.int32, shape, 0), n) == (
        lax.broadcasted_iota(jnp.int32, shape, 1) // size
    )
    pick = jnp.where(own, 1.0, 0.0).astype(BF16)
    layer_out[...] = layer_in[...]
    for h in range(heads):
        cols = slice(h * size, (h + 1) * size)
        forget = fv[0, :, cols]
        high = forget.astype(BF16).astype(F32)
        middle = (forget - high).astype(BF16).astype(F32)
        parts = jnp.concatenate([high, middle, forget - high - middle], axis=0)
        wide = lax.dot_general(
            parts.astype(BF16), pick, (((0,), (0,)), ((), ())), preferred_element_type=F32
        )
        for b in range(n):
            v = fv[1, b : b + 1, cols]
            keep = wide[:, b * size : (b + 1) * size]
            new_state[b, h] = v + keep * (state[b, h] - v)


def body(
    n_kv,
    n_tp,
    tokens,
    state,
    mix_gain,
    q_weight,
    forget_weight,
    input_weight,
    gate_weight,
    lower_bound,
    head_gain,
    out_weight,
    ffn_gain,
    ffn_gate,
    ffn_up,
    ffn_down,
):
    rows_tp, feats = tokens.shape
    rows, heads, size = state.shape[:3]
    cols = q_weight.shape[1]
    ff = ffn_gate.shape[1]
    g = rows_tp // rows
    groups = groups_of(rows)
    most = max(s for _, s in groups)
    chunk = SUB if rows % SUB == 0 else rows
    half = n_kv // 2
    square = half == 4 and cols % LANES == 0 and ff % (2 * LANES) == 0
    dims = dict(
        square=square,
        n_kv=n_kv,
        n_tp=n_tp,
        width=feats * n_kv,
        feats=feats,
        rows=rows,
        heads=heads,
        head_size=size,
        cols=cols,
        ff=ff,
        g=g,
        groups=groups,
        order=order_of(groups),
        chunk=chunk,
        chunks=rows // chunk,
    )
    per_group = 2 * n_tp + 2 * n_kv + 2 * (n_tp - 1) + 2 * half + 2 * (n_kv - 1) + 2 * n_tp + 24
    n_sems = per_group * len(groups) + 8
    dma = pltpu.SemaphoreType.DMA
    tiny = tokens.reshape(g, rows, feats)
    held = [
        pltpu.with_memory_space_constraint(x, pltpu.HBM)
        for x in (
            tiny,
            mix_gain[None, :],
            ffn_gain[None, :],
            lower_bound[None, :],
            head_gain[None, :],
            state,
            q_weight,
            forget_weight,
            input_weight,
            gate_weight,
            out_weight,
            ffn_gate,
            ffn_up,
            ffn_down,
        )
    ]
    layer_out, fv = pl.pallas_call(
        functools.partial(layer, dims),
        out_shape=(
            jax.ShapeDtypeStruct((g, rows, feats), BF16),
            jax.ShapeDtypeStruct((2, rows, cols), F32),
        ),
        in_specs=[VMEM] * 5 + [ANY] * 9,
        out_specs=(VMEM, VMEM),
        scratch_shapes=[
            pltpu.VMEM((2, 2 * feats, cols), BF16),
            pltpu.VMEM((1, 2 * feats, ff), BF16),
            pltpu.VMEM((cols, feats), BF16),
            pltpu.VMEM((ff, feats), BF16),
            pltpu.VMEM((2, n_tp, g, rows, feats), BF16),
            pltpu.VMEM((2, n_tp, g, rows, feats), BF16),
            pltpu.VMEM((n_kv * most, 2 * feats), BF16),
            pltpu.VMEM((2, 2, 1, feats), F32),
            pltpu.VMEM((n_kv, rows, 2 * cols), BF16),
            pltpu.VMEM((n_kv, rows, 2 * cols), BF16),
            pltpu.VMEM((n_kv, rows, ff), BF16),
            pltpu.VMEM((n_kv, rows, ff), BF16),
            pltpu.VMEM((2, 2, rows, cols if square else LANES), BF16),
            pltpu.VMEM((2, 2, rows, ff // 2 if square else LANES), BF16),
            pltpu.VMEM((2, n_kv, rows, LANES), F32),
            pltpu.VMEM((2, half, rows, LANES), F32),
            pltpu.VMEM((rows, cols), F32),
            pltpu.VMEM((rows, cols), F32),
            pltpu.VMEM((rows, heads, size), F32),
            pltpu.VMEM((rows, cols), F32),
            pltpu.VMEM((rows, cols), BF16),
            pltpu.VMEM((n_kv, rows, cols), BF16),
            pltpu.VMEM((rows, ff), BF16),
            pltpu.VMEM((n_kv, rows, ff), BF16),
            pltpu.VMEM((2, n_tp, g, rows, feats), F32),
            pltpu.VMEM((2, n_tp, g, rows, feats), BF16),
            pltpu.VMEM((2, n_tp, g, rows, feats), BF16),
            pltpu.VMEM((g, rows, feats), BF16),
            pltpu.VMEM((SLOTS, chunk, heads, size, size), F32),
            dma((n_sems,)),
            dma((n_sems,)),
            dma((5,)),
            dma((SLOTS,)),
        ],
        compiler_params=pltpu.CompilerParams(
            collective_id=0, has_side_effects=True, vmem_limit_bytes=VMEM_LIMIT
        ),
        name="layer",
    )(*held)
    state_block = pl.BlockSpec((chunk, heads, size, size), lambda c: (c, 0, 0, 0))
    whole = pl.BlockSpec((g, rows, feats), lambda c: (0, 0, 0))
    new_state, layer_out = pl.pallas_call(
        state_step,
        out_shape=(
            jax.ShapeDtypeStruct(state.shape, F32),
            jax.ShapeDtypeStruct((g, rows, feats), BF16),
        ),
        grid=(rows // chunk,),
        in_specs=[pl.BlockSpec((2, chunk, cols), lambda c: (0, c, 0)), whole, state_block],
        out_specs=(state_block, whole),
        compiler_params=pltpu.CompilerParams(
            dimension_semantics=("arbitrary",), vmem_limit_bytes=STATE_LIMIT
        ),
        name="state_step",
    )(fv, layer_out, state)
    return (layer_out.reshape(rows_tp, feats), new_state)


VMEM_LIMIT = 41 * 2**20
STATE_LIMIT = 20 * 2**20


def solution(mesh):
    in_specs = (
        P("tp", "kv"),
        P("kv", "tp", None, None),
        P("kv"),
        P("kv", "tp"),
        P("kv", "tp"),
        P("kv", "tp"),
        P("kv", "tp"),
        P("tp"),
        P(),
        P("tp", "kv"),
        P("kv"),
        P("kv", "tp"),
        P("kv", "tp"),
        P("tp", "kv"),
    )
    out_specs = (P("tp", "kv"), P("kv", "tp", None, None))
    step = functools.partial(body, mesh.shape["kv"], mesh.shape["tp"])
    return jax.shard_map(step, mesh=mesh, in_specs=in_specs, out_specs=out_specs, check_vma=False)
```

time: 129 us -> 87.2 us (0.68)
  Pallas kernels: 126 us -> 86.4 us
  local copies, waits for them, and re-layouts: 1.53 us -> 0.01 us
    pallas_call x2 -> x1, Pallas kernels: 106 us -> 78.1 us  [body(): pl.pallas_call(functools.partial(layer, dims), out_shape=(jax.ShapeDtypeS...]
    pallas_call x1, Pallas kernels: 20.8 us -> 8.3 us  [body(): pl.pallas_call(state_step, out_shape=(jax.ShapeDtypeStruct(state.shape, F...]
    unnamed x1 -> x2, local copies, waits for them, and re-layouts: 1.53 us -> 0.01 us
where the time goes in v1:
time: 87.2 us; the launch traced here: 87 us
  Pallas kernels  86.4 us (99%)
    pallas_call x1, Pallas kernels, body(): pl.pallas_call(functools.partial(layer, dims), out_shape=(jax.ShapeDtypeS...  78.1 us
    pallas_call x1, Pallas kernels, body(): pl.pallas_call(state_step, out_shape=(jax.ShapeDtypeStruct(state.shape, F...  8.3 us

profile of v1, /device:TPU:0, one launch (start us, length us, event | category | flops | bytes accessed | tf_op | source)
XLA Modules:
  0.0 87.0 jit_solution(16597995969079745564)
XLA Ops:
  0.6 0.0 copy-start
  0.6 78.1 %layer.1 = (bf16[2,40,512]{2,1,0:T(8,128)(2,1)S(1)}, f32[2,40,1024]{2,1,0:T(8,128)S(1)}) custom-call(bf16[2,40,512]{2,1,0:T(8,128)(2,1)} %bitcast.6, f32[1,512]{1,0:T(1,128)} %bitcast.8, f32[1,512]{1,0:T(1,128)} %bitcast.9, f32[1,1024]{1,0:T(1,128)} %bitcast.7, f32[1,128]{1,0:T(1,128)} %bitcast.10, f32[40,8,128,128]{3,2,1,0:T(8,128)} %state.1, ...), custom_call_target="tpu_custom_call" | custom-call | tf_op jit(solution)/shard_map/layer/pallas_call | solution.py:595
  78.7 0.0 copy-done
  78.7 8.3 %state_step.1 = (f32[40,8,128,128]{3,2,1,0:T(8,128)}, bf16[2,40,512]{2,1,0:T(8,128)(2,1)}) custom-call(f32[2,40,1024]{2,1,0:T(8,128)S(1)} %get-tuple-element.6.fv, bf16[2,40,512]{2,1,0:T(8,128)(2,1)S(1)} %get-tuple-element.7.layer_in, f32[40,8,128,128]{3,2,1,0:T(8,128)S(1)} %copy-done), custom_call_target="tpu_custom_call" | custom-call | tf_op jit(solution)/shard_map/state_step/pallas_call | solution.py:645
Async XLA Ops:
  0.6 78.1 %copy-start = (f32[40,8,128,128]{3,2,1,0:T(8,128)S(1)}, f32[40,8,128,128]{3,2,1,0:T(8,128)}, u32[]{:S(2)}) copy-start(f32[40,8,128,128]{3,2,1,0:T(8,128)} %state.1) | copy-start | bytes 62914564
